TPU v7x, 512 devices: a whole 4x8x8 slice. The times are simulated.
512 devices in a mesh: fs: 64 (over z, y), tp: 8 (over x, core).
Axes of the slice: x: 4, y: 8, z: 8, core: 2. Of those that a mesh axis runs over, the one named last changes fastest.
Arguments:
- tokens: bfloat16 [49152, 2048], P('fs'), may hold values from -6 to 6
- norm_gain: float32 [2048], replicated, may hold values from 0.1 to 1.9
- gate_weight: float32 [2048, 5632], P('fs', 'tp'), may hold values from -0.125 to 0.125
- up_weight: float32 [2048, 5632], P('fs', 'tp'), may hold values from -0.125 to 0.125
- gate_scale: float32 [5632], P('tp'), may hold values from 0.1 to 1.9
- up_scale: float32 [5632], P('tp'), may hold values from 0.1 to 1.9
- down_weight: float32 [5632, 2048], P('tp', 'fs'), may hold values from -0.078125 to 0.078125
- down_scale: float32 [2048], P('tp'), may hold values from 0.1 to 1.9
Outputs:
- mixed: bfloat16 [49152, 2048], P('fs', 'tp')
All inputs are finite; a program needn't handle non-finite values.
Results may differ from a plain program's by a relative error of at most 0.014.
Values may be sent and summed in bfloat16 or wider, within the bound.
A program may use at most 64 MiB of HBM per device.

v0:
```python
import jax
import jax.numpy as jnp
from jax import lax
from jax.sharding import Mesh
from jax.sharding import PartitionSpec as P

FS = ("fs_0", "fs_1")


def sent_together(arrays, axis, dim, along):
    both = jnp.concatenate(arrays, axis=along)
    out, at, done = (lax.all_gather(both, axis, axis=dim, tiled=True), 0, [])
    for a in arrays:
        done.append(lax.slice_in_dim(out, at, at + a.shape[along], axis=along))
        at += a.shape[along]
    return tuple(done)


def joined_along(blocks, dim):
    lengths = list(blocks.shape[1:])
    lengths[dim] *= blocks.shape[0]
    return jnp.moveaxis(blocks, 0, dim).reshape(lengths)


def stacked_from(array, axes, sequence):
    blocks = array
    for k in sequence:
        blocks = lax.all_gather(blocks, axes[k])
    done = sequence[::-1]
    back = [done.index(k) for k in range(len(axes))]
    blocks = blocks.transpose(*back, *range(len(axes), blocks.ndim))
    return blocks.reshape(-1, *array.shape)


def whole_of(array, axes, sequence, dim):
    return joined_along(stacked_from(array, axes, sequence), dim)


def body(tokens, norm_gain, gate_weight, up_weight, gate_scale, up_scale, down_weight, down_scale):
    values = tokens.astype(jnp.float32)
    normed = (
        values * lax.rsqrt(jnp.mean(values * values, axis=-1, keepdims=True) + 1e-06) * norm_gain
    ).astype(jnp.bfloat16)
    gate_low = gate_weight.astype(jnp.bfloat16)
    up_low = up_weight.astype(jnp.bfloat16)
    down_low = down_weight.astype(jnp.bfloat16)

    def add_rows(piece):
        return jnp.dot(normed, piece, preferred_element_type=jnp.float32)

    pieces = sent_together((gate_low, up_low), FS, 0, 1)
    gate = add_rows(pieces[0])
    up = add_rows(pieces[1])
    hidden = (jax.nn.silu(gate * gate_scale) * (up * up_scale)).astype(jnp.bfloat16)
    terms = jnp.dot(hidden, whole_of(down_low, FS, (0, 1), 1), preferred_element_type=jnp.float32)
    summed = lax.psum_scatter(
        terms.astype(jnp.bfloat16), "tp", scatter_dimension=1, tiled=True
    ).astype(jnp.float32)
    return (summed * down_scale).astype(jnp.bfloat16)


def solution(mesh):
    split = Mesh(mesh.devices.reshape(8, 8, mesh.shape["tp"]), ("fs_0", "fs_1", "tp"))
    placed = (P(FS, None), P(), P(FS, "tp"), P(FS, "tp"), P("tp"), P("tp"), P("tp", FS), P("tp"))
    return jax.shard_map(body, mesh=split, in_specs=placed, out_specs=P(FS, "tp"), check_vma=False)
```

profile of v0, /device:TPU:8, one launch (start us, length us, event | category | flops | bytes accessed | tf_op | source)
XLA Modules:
  0.0 243.1 jit_solution(6099476266677062072)
XLA Ops:
  6.5 0.0 all-gather.8.cloned.1.call-start
  6.5 0.9 convert_bitcast_fusion
  7.4 33.6 %all-gather.2 = bf16[8,704,32]{1,2,0:T(8,128)(2,1)} all-gather(bf16[1,704,32]{1,2,0:T(8,128)(2,1)S(1)} %convert_bitcast_fusion), channel_id=2, replica_groups=mesh['fs_0'=8,'fs_1'=8,'tp'=8] {'fs_0'}, dimensions={0}, use_global_device_ids=true | all-gather | bytes 405504 | tf_op jit(solution)/shard_map/all_gather | solution.py:28
  41.0 0.0 all-gather.8.cloned.1.call-update
  41.1 0.0 all-gather.6.cloned.1.call-start
  41.1 0.9 convert_element_type.29
  42.0 0.9 convert_element_type.30
  42.9 0.7 pad_maximum_fusion
  43.6 0.0 all-gather.6.cloned.1.call-update
  43.7 0.0 reduce-scatter.2.cloned.1.call-start
  43.7 2.6 %fusion = f32[768]{0:T(1024)S(1)} fusion(bf16[768,2048]{1,0:T(8,128)(2,1)} %param.8), kind=kLoop, calls=%fused_computation.2 | loop fusion | flops 4717824 | bytes 3148800 | tf_op jit(solution)/shard_map/reduce_sum | solution.py:42
  46.3 39.9 %all-gather.8.cloned.1.call-done = bf16[64,704,32]{1,2,0:T(8,128)(2,1)} async-done(((bf16[8,704,32]{1,2,0:T(8,128)(2,1)}), bf16[64,704,32]{1,2,0:T(8,128)(2,1)}) %all-gather.8.cloned.1.call-update) | async-done | bytes 2883600 | tf_op jit(solution)/shard_map/all_gather | solution.py:28
  86.2 0.0 copy-start
  86.2 0.0 copy-start.2
  86.2 4.0 %copy.10 = bf16[8,8,704,32]{2,3,1,0:T(8,128)(2,1)} copy(bf16[8,8,704,32]{2,3,0,1:T(8,128)(2,1)} %bitcast.11) | data formatting | bytes 5767168 | tf_op jit(solution)/shard_map/transpose | solution.py:31
  90.2 0.0 copy-start.3
  90.2 0.0 copy-start.4
  90.2 88.0 %all-gather.6.cloned.1.call-done = bf16[2048,1408]{1,0:T(8,128)(2,1)} async-done(((bf16[32,1408]{1,0:T(8,128)(2,1)}), bf16[2048,1408]{1,0:T(8,128)(2,1)}) %all-gather.6.cloned.1.call-update) | async-done | bytes 5767184 | tf_op jit(solution)/shard_map/all_gather | solution.py:12
  178.2 0.0 copy-done
  178.2 0.0 copy-done.2
  178.2 7.0 %fusion.3 = f32[768,704]{0,1:T(8,128)} fusion(bf16[2048,1408]{1,0:T(8,128)(2,1)} %all-gather.6.cloned.1.call-done, bf16[768,2048]{1,0:T(8,128)(2,1)S(1)} %copy-done, f32[2048]{0:T(1024)S(1)} %copy-done.2, f32[768]{0:T(1024)S(1)} %add_rsqrt_fusion), kind=kOutput, calls=%fused_computation.6 | convolution fusion | flops 2220883968 | bytes 8465408 | tf_op jit(solution)/shard_map/dot_general | solution.py:49
  185.2 0.0 copy-done.3
  185.2 0.0 copy-done.4
  185.2 11.9 %convolution_convert_fusion = bf16[768,2048]{1,0:T(8,128)(2,1)} fusion(bf16[704,2048]{0,1:T(8,128)(2,1)} %bitcast.12, f32[768,704]{0,1:T(8,128)} %fusion.3, bf16[2048,1408]{1,0:T(8,128)(2,1)} %all-gather.6.cloned.1.call-done, f32[704]{0:T(1024)S(1)} %copy-done.3, f32[704]{0:T(1024)S(1)} %copy-done.4, bf16[768,2048]{1,0:T(8,128)(2,1)S(1)} %copy-done, ...), kind=kOutput, calls=%fused_computation.5 | convolution fusion | flops 4441374720 | bytes 14762496 | tf_op jit(solution)/shard_map/dot_general | solution.py:55
  197.0 0.0 copy-start.1
  197.0 0.0 reduce-scatter.2.cloned.1.call-update
  197.1 37.7 %reduce-scatter.2.cloned.1.call-done = bf16[768,256]{1,0:T(8,128)(2,1)} async-done(((bf16[768,2048]{1,0:T(8,128)(2,1)}), bf16[768,256]{1,0:T(8,128)(2,1)}) %reduce-scatter.2.cloned.1.call-update) | async-done | bytes 393232 | tf_op jit(solution)/shard_map/reduce_scatter | solution.py:56
  234.8 0.0 copy-done.1
  234.8 1.8 multiply_convert_fusion.1
  (1 shorter events, 0.0 us)
Async XLA Ops:
  6.5 79.6 %all-gather.8.cloned.1.call-start = ((), (), s32[]{:S(2)}) async-start(), calls=%async_computation.3 | async-start | bytes 3538944 | tf_op jit(solution)/shard_map/all_gather | solution.py:28
  41.1 137.1 %all-gather.6.cloned.1.call-start = ((), (), s32[]{:S(2)}) async-start(), calls=%async_computation.1 | async-start | bytes 5857280 | tf_op jit(solution)/shard_map/all_gather | solution.py:12
  43.7 191.1 %reduce-scatter.2.cloned.1.call-start = ((), (), s32[]{:S(2)}) async-start(), calls=%async_computation.2 | async-start | bytes 3538944 | tf_op jit(solution)/shard_map/reduce_scatter | solution.py:56
  86.2 92.0 %copy-start = (bf16[768,2048]{1,0:T(8,128)(2,1)S(1)}, bf16[768,2048]{1,0:T(8,128)(2,1)}, u32[]{:S(2)}) copy-start(bf16[768,2048]{1,0:T(8,128)(2,1)} %param.8) | copy-start | bytes 9437188
  86.2 92.0 %copy-start.2 = (f32[2048]{0:T(1024)S(1)}, f32[2048]{0:T(1024)}, u32[]{:S(2)}) copy-start(f32[2048]{0:T(1024)} %param.9) | copy-start | bytes 24580
  90.2 94.9 %copy-start.3 = (f32[704]{0:T(1024)S(1)}, f32[704]{0:T(1024)}, u32[]{:S(2)}) copy-start(f32[704]{0:T(1024)} %param.13) | copy-start | bytes 8452
  90.2 94.9 %copy-start.4 = (f32[704]{0:T(1024)S(1)}, f32[704]{0:T(1024)}, u32[]{:S(2)}) copy-start(f32[704]{0:T(1024)} %param.12) | copy-start | bytes 8452
  197.0 37.8 %copy-start.1 = (f32[256]{0:T(256)S(1)}, f32[256]{0:T(256)}, u32[]{:S(2)}) copy-start(f32[256]{0:T(256)} %param.15) | copy-start | bytes 3076
Sparse Core Ops, SparseCore 0:
  41.2 44.9 all-gather.7
  89.2 88.9 all-gather.5
  197.2 37.5 reduce-scatter.1
where the time goes:
time: 243 us
  waiting for transfers between devices  166 us (68%)
  blocking collectives  33.6 us (14%)
  matrix products  18.8 us (8%)
  between operations  13.1 us (5%)
  other arithmetic  7.81 us (3%)
  local copies, waits for them, and re-layouts  4.05 us (2%)
    all_gather x1, waiting for transfers between devices, sent_together(): out, at, done = (lax.all_gather(both, axis, axis=dim, tiled=True), 0, [])  88 us
    all_gather x1, waiting for transfers between devices, stacked_from(): blocks = lax.all_gather(blocks, axes[k])  39.9 us
    reduce_scatter x1, waiting for transfers between devices, body(): lax.psum_scatter(terms.astype(jnp.bfloat16), 'tp', scatter_dimension=1, t...  37.7 us
    all_gather x1, blocking collectives, stacked_from(): blocks = lax.all_gather(blocks, axes[k])  33.6 us
    dot_general x1, matrix products, body(): jnp.dot(hidden, whole_of(down_low, FS, (0, 1), 1), preferred_element_type...  11.9 us
    dot_general x1, matrix products, add_rows(): return jnp.dot(normed, piece, preferred_element_type=jnp.float32)  6.96 us
  transfers between devices with their start and end apart: 3, of which 3 were waited for; matrix products, arithmetic and copies ran while one was open for 4% of the time, Pallas kernels for 0%

commit v1 on v0

v1 whole, which is shorter than its diff:
```python
import jax
import jax.numpy as jnp
from jax import lax
from jax.experimental import pallas as pl
from jax.experimental.pallas import tpu as pltpu
from jax.sharding import Mesh
from jax.sharding import PartitionSpec as P

FS = ("fs_0", "fs_1")
MESH = pl.DeviceIdType.MESH
F32, BF16 = jnp.float32, jnp.bfloat16
OFF = (0, 1, -1, 2, -2, 3, -3, 4)
PLUS, MINUS = 0, 1


def wrap(i):
    return lax.rem(i + 16, 8)


class Gather:
    def __init__(self, buf, major_axis, minor_axis, major, minor, sems):
        self.buf, self.major_axis, self.minor_axis = buf, major_axis, minor_axis
        self.major, self.minor = major, minor
        self.send1, self.send2, self.recv1, self.recv2 = sems

    def first(self, way, step, source):
        at = self.buf.at[self.major, wrap(self.minor + source)]
        to = wrap(self.minor + (1 if way == PLUS else -1))
        return pltpu.make_async_remote_copy(
            src_ref=at, dst_ref=at, send_sem=self.send1, recv_sem=self.recv1.at[way, step - 1],
            device_id={self.minor_axis: to}, device_id_type=MESH,
        )

    def second(self, way, hop, j, source):
        at = self.buf.at[wrap(self.major + source), wrap(self.minor + OFF[j])]
        to = wrap(self.major + (1 if way == PLUS else -1))
        return pltpu.make_async_remote_copy(
            src_ref=at, dst_ref=at, send_sem=self.send2, recv_sem=self.recv2.at[way, hop - 1, j],
            device_id={self.major_axis: to}, device_id_type=MESH,
        )

    def start_first(self):
        self.first(PLUS, 1, 0).start()
        self.first(MINUS, 1, 0).start()

    def start_second(self, j):
        self.second(PLUS, 1, j, 0).start()
        self.second(MINUS, 1, j, 0).start()

    def line(self, step):
        self.first(PLUS, step, -step).wait_recv()
        if step < 4:
            self.first(PLUS, step + 1, -step).start()
            self.first(MINUS, step, step).wait_recv()
        if step < 3:
            self.first(MINUS, step + 1, step).start()

    def hop(self, hop, j):
        for way, side, last in ((PLUS, -1, j < 4), (MINUS, 1, j >= 4)):
            self.second(way, hop, j, side * hop).wait_recv()
            if last:
                self.second(way, hop + 1, j, side * hop).start()
            else:
                @pl.when(hop < 3)
                def _():
                    self.second(way, hop + 1, j, side * hop).start()

    def last(self, j):
        if j < 4:
            self.second(PLUS, 4, j, -4).wait_recv()
        else:
            self.second(MINUS, 4, j, 4).wait_recv()

    def drain(self):
        one = self.buf.at[0, pl.ds(0, 7)]
        many = self.buf.at[pl.ds(0, 7)]
        for ref, sem in ((one, self.send1), (many, self.send2)):
            pltpu.make_async_copy(ref, ref, sem).wait()


def kernel(
    tokens, gain, gate_w, up_w, gate_s, up_s, down_w, down_s, out,
    tok, x_a, x_b, buf_a, buf_b, buf_c, buf_d, acc_a, acc_b, hid,
    own_a, own_b, give_a, give_b, got_a, got_b, sum_a, sum_b, all_a, all_b, flat,
    tok_sem, send1, send2, recv1, recv2, pair_send, pair_a, pair_b, x_send, x_a_sem, x_b_sem,
):
    z, y, tp = lax.axis_index("fs_0"), lax.axis_index("fs_1"), lax.axis_index("tp")
    core = lax.rem(tp, 2)
    other = 1 - core
    peer = tp + 1 - 2 * core

    fetch = pltpu.make_async_copy(tokens, tok, tok_sem)
    fetch.start()

    barrier = pltpu.get_barrier_semaphore()
    for axis, me in (("fs_0", z), ("fs_1", y)):
        for side in (1, -1):
            pl.semaphore_signal(barrier, inc=1, device_id={axis: wrap(me + side)}, device_id_type=MESH)
    for k in range(1, 8):
        pl.semaphore_signal(barrier, inc=1, device_id={"tp": lax.rem(tp + k, 8)}, device_id_type=MESH)

    gw, uw = gate_w[...].astype(BF16), up_w[...].astype(BF16)
    tails = jnp.concatenate([gw[:, 640:], uw[:, 640:]], axis=1)
    buf_a[z, y, :, 0:640] = gw[:, 0:640]
    buf_a[z, y, :, 640:768] = uw[:, 0:128]
    buf_b[y, z, :, 0:512] = uw[:, 128:640]
    buf_b[y, z, :, 512:640] = tails

    def sems(k):
        return send1.at[k], send2.at[k], recv1.at[k], recv2.at[k]

    ga = Gather(buf_a, "fs_0", "fs_1", z, y, sems(0))
    gb = Gather(buf_b, "fs_1", "fs_0", y, z, sems(1))
    gc = Gather(buf_c, "fs_0", "fs_1", z, y, sems(2))
    gd = Gather(buf_d, "fs_1", "fs_0", y, z, sems(3))
    wide, deep = (ga, gb), (gc, gd)

    pl.semaphore_wait(barrier, 11)
    for g in wide:
        g.start_first()
    for g in wide:
        g.start_second(0)

    eye = (lax.broadcasted_iota(jnp.int32, (32, 32), 0) == lax.broadcasted_iota(jnp.int32, (32, 32), 1)).astype(BF16)
    turned = lax.dot_general(
        eye, down_w[...].astype(BF16), (((1,), (1,)), ((), ())), preferred_element_type=F32
    )
    turned = jnp.concatenate([turned, jnp.zeros((32, 64), F32)], axis=1).astype(BF16)
    buf_c[z, y] = turned[0:16]
    buf_d[y, z] = turned[16:32]

    acc_a[...] = jnp.zeros_like(acc_a)
    acc_b[...] = jnp.zeros_like(acc_b)
    fetch.wait()

    def prepare(k, _):
        rows = pl.ds(pl.multiple_of(k * 64, 64), 64)
        values = tok[rows, :].astype(F32)
        normed = values * lax.rsqrt(jnp.mean(values * values, axis=-1, keepdims=True) + 1e-06) * gain[...]
        for b in range(8):
            x_a[b, rows, :] = normed[:, b * 256 : b * 256 + 256].astype(BF16)
        lane = lax.broadcasted_iota(jnp.int32, (64, 128), 1) // 32
        for yy in range(8):
            for zh in range(2):
                tile = None
                for zl in range(4):
                    t = (zh * 4 + zl) * 2 + yy // 4
                    piece = normed[:, t * 128 : t * 128 + 128]
                    shift = ((zl - yy % 4) * 32) % 128
                    if shift:
                        piece = pltpu.roll(piece, shift, 1)
                    tile = piece if tile is None else jnp.where(lane == zl, piece, tile)
                x_b[yy, rows, zh * 128 : zh * 128 + 128] = tile.astype(BF16)
        return 0

    for step in range(1, 5):
        for g in wide:
            g.line(step)
        for g in wide:
            g.start_second(2 * step - 1)
            if step < 4:
                g.start_second(2 * step)
        lax.fori_loop((step - 1) * 3, step * 3, prepare, 0)

    for g in deep:
        g.start_first()

    def wide_piece(p, away):
        block, half = p // 2, p % 2
        sign = 1 if block % 2 == 0 else -1
        rows = slice(half * 384, half * 384 + 384)
        if block < 2:
            at = wrap(z + sign * away)
            acc_a[rows, :] += jnp.dot(
                x_a[at, rows, :], buf_a[at].reshape(256, 768), preferred_element_type=F32
            )
        else:
            at = wrap(y + sign * away)
            acc_b[rows, :] += jnp.dot(
                x_b[at, rows, :], buf_b[at].reshape(256, 640), preferred_element_type=F32
            )

    def wide_round(hop, _):
        for j in range(8):
            for g in wide:
                g.hop(hop, j)
            if (j // 2) % 2 == 0:
                wide_piece(j, hop - 1)
            else:
                @pl.when(hop > 1)
                def _():
                    wide_piece(j, hop - 1)
        for step in range(1, 4):
            @pl.when(hop == step)
            def _():
                for g in deep:
                    g.line(step)
        return 0

    lax.fori_loop(1, 4, wide_round, 0)
    for g in deep:
        g.line(4)
    for j in range(8):
        for g in deep:
            g.start_second(j)
    for j in range(8):
        wide_piece(j, 3)
        for g in wide:
            g.last(j)
    for j in (0, 1, 4, 5):
        wide_piece(j, 4)

    def activate(k, _):
        rows = pl.ds(pl.multiple_of(k * 128, 128), 128)
        gate_at, up_at = gate_s[...], up_s[...]
        left, right = acc_a[rows, :], acc_b[rows, :]
        tail = right[:, 512:640]
        g = jnp.concatenate([left[:, 0:640], tail], axis=1) * gate_at
        u = jnp.concatenate([left[:, 640:768], right[:, 0:512], pltpu.roll(tail, 64, 1)], axis=1) * up_at
        h = g / (1.0 + jnp.exp(-g)) * u
        lane = lax.broadcasted_iota(jnp.int32, h.shape, 1)
        h = jnp.where(lane < 704, h, 0.0)
        hid[k] = h.T.astype(BF16)
        return 0

    lax.fori_loop(0, 6, activate, 0)

    def half_of(which):
        return jnp.concatenate([hid[which * 3 + k] for k in range(3)], axis=1)

    def pair(group, at):
        give, got, sem = (give_a, got_a, pair_a) if group == 0 else (give_b, got_b, pair_b)
        return pltpu.make_async_remote_copy(
            src_ref=give.at[at], dst_ref=got.at[at], send_sem=pair_send.at[group], recv_sem=sem.at[at],
            device_id={"tp": peer}, device_id_type=MESH,
        )

    def deep_piece(p, away):
        block, mine = p % 4, p // 4
        sign = 1 if block % 2 == 0 else -1
        group = block // 2
        at = wrap((z, y)[group] + sign * away)
        left = (buf_c, buf_d)[group][at].reshape(128, 768)
        part = jnp.dot(left, half_of(core if mine else other), preferred_element_type=F32)
        if mine:
            (own_a, own_b)[group][at] = part
        else:
            (give_a, give_b)[group][at] = part.astype(BF16)
            pair(group, at).start()

    def to_owner_a(at):
        return pltpu.make_async_remote_copy(
            src_ref=sum_a.at[at], dst_ref=all_a.at[tp], send_sem=x_send.at[0], recv_sem=x_a_sem.at[tp],
            device_id={"tp": at}, device_id_type=MESH,
        )

    def to_owner_b(at, owner):
        return pltpu.make_async_remote_copy(
            src_ref=sum_b.at[at, owner], dst_ref=all_b.at[tp, at], send_sem=x_send.at[1], recv_sem=x_b_sem.at[tp],
            device_id={"tp": owner}, device_id_type=MESH,
        )

    def combine(group, at):
        pair(group, at).wait_recv()
        if group == 0:
            total = (own_a[at] + got_a[at].astype(F32)).astype(BF16).reshape(8, 16, 384)

            @pl.when(at == tp)
            def _():
                all_a[tp] = total

            @pl.when(at != tp)
            def _():
                sum_a[at] = total
                to_owner_a(at).start()
        else:
            sum_b[at] = (own_b[at] + got_b[at].astype(F32)).astype(BF16).reshape(8, 16, 384)
            for k in range(1, 8):
                to_owner_b(at, lax.rem(tp + k, 8)).start()
            all_b[tp, at] = sum_b[at, tp]

    def combine_all(away, both):
        for group, me in ((0, z), (1, y)):
            combine(group, wrap(me + away))
            if both is True:
                combine(group, wrap(me - away))
            elif both is not False:
                @pl.when(both)
                def _():
                    combine(group, wrap(me - away))

    def deep_round(hop, _):
        for j in range(8):
            for g in deep:
                g.hop(hop, j)
            if j % 2 == 0:
                deep_piece(j, hop - 1)
            else:
                @pl.when(hop > 1)
                def _():
                    deep_piece(j, hop - 1)
        combine_all(hop - 1, hop > 1)
        return 0

    lax.fori_loop(1, 4, deep_round, 0)
    for j in range(8):
        for g in deep:
            g.last(j)
        deep_piece(j, 3)
    combine_all(3, True)
    for j in (0, 2, 4, 6):
        deep_piece(j, 4)
    combine_all(4, False)

    for k in range(1, 8):
        source = lax.rem(tp + k, 8)
        pltpu.make_async_copy(all_a.at[source], all_a.at[source], x_a_sem.at[source]).wait()
        pltpu.make_async_copy(all_b.at[source], all_b.at[source], x_b_sem.at[source]).wait()

    for h, held in ((0, all_a), (1, all_b)):
        for c in range(2):
            total = held[c].astype(F32)
            for k in range(1, 4):
                total += held[2 * k + c].astype(F32)
            flat[:, h, :, c * 384 : c * 384 + 384] = total
    scale = down_s[...]
    for k in range(6):
        lanes = slice(k * 128, k * 128 + 128)
        block = flat[:, :, :, lanes].reshape(256, 128)
        out[lanes, :] = (block.T * scale).astype(BF16)

    for g in wide + deep:
        g.drain()
    for group, ref in ((0, give_a), (1, give_b)):
        pltpu.make_async_copy(ref, ref, pair_send.at[group]).wait()
    few = sum_a.at[pl.ds(0, 7)]
    pltpu.make_async_copy(few, few, x_send.at[0]).wait()
    few = sum_b.at[:, pl.ds(0, 7)]
    pltpu.make_async_copy(few, few, x_send.at[1]).wait()


def body(tokens, norm_gain, gate_weight, up_weight, gate_scale, up_scale, down_weight, down_scale):
    def padded(v):
        return jnp.pad(v, (0, 64), constant_values=1.0).reshape(1, 768)

    vmem = pl.BlockSpec(memory_space=pltpu.VMEM)
    hbm = pl.BlockSpec(memory_space=pl.ANY)
    dma = pltpu.SemaphoreType.DMA
    return pl.pallas_call(
        kernel,
        out_shape=jax.ShapeDtypeStruct((768, 256), BF16),
        in_specs=[hbm] + [vmem] * 7,
        out_specs=vmem,
        scratch_shapes=[
            pltpu.VMEM((768, 2048), BF16),
            pltpu.VMEM((8, 768, 256), BF16),
            pltpu.VMEM((8, 768, 256), BF16),
            pltpu.VMEM((8, 8, 32, 768), BF16),
            pltpu.VMEM((8, 8, 32, 640), BF16),
            pltpu.VMEM((8, 8, 16, 768), BF16),
            pltpu.VMEM((8, 8, 16, 768), BF16),
            pltpu.VMEM((768, 768), F32),
            pltpu.VMEM((768, 640), F32),
            pltpu.VMEM((6, 768, 128), BF16),
            pltpu.VMEM((8, 128, 384), F32),
            pltpu.VMEM((8, 128, 384), F32),
            pltpu.VMEM((8, 128, 384), BF16),
            pltpu.VMEM((8, 128, 384), BF16),
            pltpu.VMEM((8, 128, 384), BF16),
            pltpu.VMEM((8, 128, 384), BF16),
            pltpu.VMEM((8, 8, 16, 384), BF16),
            pltpu.VMEM((8, 8, 16, 384), BF16),
            pltpu.VMEM((8, 8, 16, 384), BF16),
            pltpu.VMEM((8, 8, 16, 384), BF16),
            pltpu.VMEM((8, 2, 16, 768), F32),
            dma,
            dma((4,)),
            dma((4,)),
            dma((4, 2, 4)),
            dma((4, 2, 4, 8)),
            dma((2,)),
            dma((8,)),
            dma((8,)),
            dma((2,)),
            dma((8,)),
            dma((8,)),
        ],
        compiler_params=pltpu.CompilerParams(
            collective_id=0, has_side_effects=True, vmem_limit_bytes=56 * 1024 * 1024
        ),
    )(
        tokens, norm_gain.reshape(1, 2048), gate_weight, up_weight, padded(gate_scale), padded(up_scale),
        down_weight, down_scale.reshape(1, 256),
    )


def solution(mesh):
    split = Mesh(mesh.devices.reshape(8, 8, mesh.shape["tp"]), ("fs_0", "fs_1", "tp"))
    placed = (P(FS, None), P(), P(FS, "tp"), P(FS, "tp"), P("tp"), P("tp"), P("tp", FS), P("tp"))
    return jax.shard_map(body, mesh=split, in_specs=placed, out_specs=P(FS, "tp"), check_vma=False)
```

time: 243 us -> 95.9 us (0.39)
  the two profiles are of different devices: /device:TPU:8 before, /device:TPU:5 now
where the time goes in v1:
time: 95.9 us; the launch traced here: 95.7 us
  Pallas kernels  89.5 us (93%)
  local copies, waits for them, and re-layouts  6.12 us (6%)
    pallas_call x1, Pallas kernels, body(): pl.pallas_call(kernel, out_shape=jax.ShapeDtypeStruct((768, 256), BF16),...  89.5 us
    unnamed x2, local copies, waits for them, and re-layouts  3.56 us

profile of v1, /device:TPU:5, one launch (start us, length us, event | category | flops | bytes accessed | tf_op | source)
XLA Modules:
  0.0 95.7 jit_solution(15512450514966171731)
XLA Ops:
  0.0 0.7 pad.7
  0.7 0.6 reshape.13.gate_s
  1.3 0.7 pad.8
  2.0 0.6 reshape.14.up_s
  2.6 1.8 %copy.9.down_w = f32[704,32]{1,0:T(8,128)} copy(f32[704,32]{0,1:T(8,128)} %param.14) | data formatting | bytes 180224 | tf_op args[6]
  4.4 89.5 %shard_map.82 = bf16[768,256]{1,0:T(8,128)(2,1)} custom-call(bf16[768,2048]{1,0:T(8,128)(2,1)} %tokens.1, f32[1,2048]{1,0:T(1,128)} %bitcast.2, f32[32,704]{1,0:T(8,128)} %gate_w.1, f32[32,704]{1,0:T(8,128)} %up_w.1, f32[1,768]{1,0:T(1,128)} %reshape.13.gate_s, f32[1,768]{1,0:T(1,128)} %reshape.14.up_s, f32[704,32]{1,0:T(8,128)} %copy.9.down_w, f32[1,256]{1,0:T(1,128)} %bitcast.3), custom_call_target="tpu_custom_call" | custom-call | tf_op jit(solution)/shard_map/pallas_call | solution.py:349
  93.9 1.8 %copy.11 = bf16[768,256]{1,0:T(8,128)(2,1)} copy(bf16[768,256]{1,0:T(8,128)(2,1)} %shard_map.82) | data formatting | bytes 786432

commit v2 on v1

v2 whole, which is shorter than its diff:
```python
import jax
import jax.numpy as jnp
from jax import lax
from jax.experimental import pallas as pl
from jax.experimental.pallas import tpu as pltpu
from jax.sharding import Mesh
from jax.sharding import PartitionSpec as P

FS = ("fs_0", "fs_1")
MESH = pl.DeviceIdType.MESH
F32, BF16 = jnp.float32, jnp.bfloat16
OFF = (0, 1, -1, 2, -2, 3, -3, 4)
PLUS, MINUS = 0, 1


def wrap(i):
    return lax.rem(i + 16, 8)


class Gather:
    def __init__(self, buf, major, minor, along_major, along_minor, sems):
        self.buf, self.major, self.minor = buf, major, minor
        self.along_major, self.along_minor = along_major, along_minor
        self.send1, self.send2, self.recv1, self.recv2 = sems

    def first(self, way, step, source):
        at = self.buf.at[self.major, wrap(self.minor + source)]
        return pltpu.make_async_remote_copy(
            src_ref=at, dst_ref=at, send_sem=self.send1, recv_sem=self.recv1.at[way, step - 1],
            device_id=self.along_minor[way], device_id_type=MESH,
        )

    def second(self, way, hop, j, source):
        at = self.buf.at[wrap(self.major + source), wrap(self.minor + OFF[j])]
        return pltpu.make_async_remote_copy(
            src_ref=at, dst_ref=at, send_sem=self.send2, recv_sem=self.recv2.at[way, hop - 1, j],
            device_id=self.along_major[way], device_id_type=MESH,
        )

    def start_first(self):
        self.first(PLUS, 1, 0).start()
        self.first(MINUS, 1, 0).start()

    def start_second(self, j):
        self.send(PLUS, j)
        self.send(MINUS, j)

    def send(self, way, j):
        self.second(way, 1, j, 0).start()

    def line(self, step):
        self.first(PLUS, step, -step).wait_recv()
        if step < 4:
            self.first(PLUS, step + 1, -step).start()
            self.first(MINUS, step, step).wait_recv()
        if step < 3:
            self.first(MINUS, step + 1, step).start()

    def hop(self, hop, j):
        for way, side, last in ((PLUS, -1, j < 4), (MINUS, 1, j >= 4)):
            self.second(way, hop, j, side * hop).wait_recv()
            if last or not isinstance(hop, int) or hop < 3:
                self.second(way, hop + 1, j, side * hop).start()

    def last(self, j):
        if j < 4:
            self.second(PLUS, 4, j, -4).wait_recv()
        else:
            self.second(MINUS, 4, j, 4).wait_recv()

    def drain(self):
        one = self.buf.at[0, pl.ds(0, 7)]
        many = self.buf.at[pl.ds(0, 7)]
        for ref, sem in ((one, self.send1), (many, self.send2)):
            pltpu.make_async_copy(ref, ref, sem).wait()


def kernel(
    tokens, gain, gate_w, up_w, gate_s, up_s, down_w, down_s, out,
    tok, gw_in, uw_in, dw_in, x_all, buf_a, buf_b, buf_c, buf_d, acc_a, acc_b, hid,
    own_a, own_b, give_a, give_b, got_a, got_b, sum_a, sum_b, via_a, via_b, all_a, all_b, flat,
    in_sem, send1, send2, recv1, recv2, pair_send, pair_a, pair_b, via_a_sem, via_b_sem, x_send, x_a_sem, x_b_sem,
):
    z, y, tp = lax.axis_index("fs_0"), lax.axis_index("fs_1"), lax.axis_index("tp")
    core = lax.rem(tp, 2)
    other = 1 - core
    peer = tp + 1 - 2 * core
    chip = tp // 2
    onward = 1 - 2 * core

    def place(step, c):
        return 2 * lax.rem(chip + step + 8, 4) + c

    along_z = [(wrap(z + side), y, tp) for side in (1, -1)]
    along_y = [(z, wrap(y + side), tp) for side in (1, -1)]
    barrier = pltpu.get_barrier_semaphore()
    near = along_z + along_y + [(z, y, peer)] + [(z, y, place(step, c)) for step in (1, 3) for c in (0, 1)]
    for device in near:
        pl.semaphore_signal(barrier, inc=1, device_id=device, device_id_type=MESH)

    fetches = [
        pltpu.make_async_copy(src, dst, in_sem.at[k])
        for k, (src, dst) in enumerate(((gate_w, gw_in), (up_w, uw_in), (down_w, dw_in), (tokens, tok)))
    ]
    for fetch in fetches:
        fetch.start()

    major = z + core * (y - z)
    minor = y + core * (z - y)

    def either(first, second):
        return [tuple(f + core * (s - f) for f, s in zip(one, two)) for one, two in zip(first, second)]

    along_major, along_minor = either(along_z, along_y), either(along_y, along_z)

    def sems(k):
        return send1.at[k], send2.at[k], recv1.at[k], recv2.at[k]

    ga = Gather(buf_a, major, minor, along_major, along_minor, sems(0))
    gb = Gather(buf_b, minor, major, along_minor, along_major, sems(1))
    gc = Gather(buf_c, z, y, along_z, along_y, sems(2))
    gd = Gather(buf_d, y, z, along_y, along_z, sems(3))
    wide, deep = (ga, gb), (gc, gd)

    fetches[0].wait()
    fetches[1].wait()
    gw, uw = gw_in[...].astype(BF16), uw_in[...].astype(BF16)
    buf_a[major, minor, :, 0:640] = gw[:, 0:640]
    buf_a[major, minor, :, 640:768] = uw[:, 0:128]
    buf_b[minor, major, :, 0:512] = uw[:, 128:640]
    buf_b[minor, major, :, 512:640] = jnp.concatenate([gw[:, 640:], uw[:, 640:]], axis=1)
    fetches[2].wait()
    turned = jnp.concatenate([dw_in[...], jnp.zeros((32, 64), F32)], axis=1).astype(BF16)
    buf_c[z, y] = turned[0:16]
    buf_d[y, z] = turned[16:32]

    pl.semaphore_wait(barrier, len(near))
    for g in wide + deep:
        g.start_first()
    for g in wide:
        g.start_second(0)

    acc_a[...] = jnp.zeros_like(acc_a)
    acc_b[...] = jnp.zeros_like(acc_b)
    fetches[3].wait()

    def prepare(k, _):
        rows = pl.ds(pl.multiple_of(k * 16, 16), 16)
        values = tok[rows, :].astype(F32)
        normed = values * lax.rsqrt(jnp.mean(values * values, axis=-1, keepdims=True) + 1e-06) * gain[...]
        for b in range(8):
            x_all[0, b, rows, :] = normed[:, b * 256 : b * 256 + 256].astype(BF16)
        lane = lax.broadcasted_iota(jnp.int32, (16, 128), 1) // 32
        for yy in range(8):
            for zh in range(2):
                tile = None
                for zl in range(4):
                    t = (zh * 4 + zl) * 2 + yy // 4
                    piece = normed[:, t * 128 : t * 128 + 128]
                    shift = ((zl - yy % 4) * 32) % 128
                    if shift:
                        piece = pltpu.roll(piece, shift, 1)
                    tile = piece if tile is None else jnp.where(lane == zl, piece, tile)
                x_all[1, yy, rows, zh * 128 : zh * 128 + 128] = tile.astype(BF16)
        return 0

    for step in range(1, 5):
        for g in wide + deep:
            g.line(step)
        for g in wide:
            g.start_second(2 * step - 1)
            if step < 4:
                g.start_second(2 * step)
        lax.fori_loop((step - 1) * 12, step * 12, prepare, 0)

    def wide_piece(p, away):
        block, half = p // 2, p % 2
        sign = 1 if block % 2 == 0 else -1
        rows = slice(half * 384, half * 384 + 384)
        if block < 2:
            at = wrap(major + sign * away)
            acc_a[rows, :] += jnp.dot(
                x_all[core, at, rows, :], buf_a[at].reshape(256, 768), preferred_element_type=F32
            )
        else:
            at = wrap(minor + sign * away)
            acc_b[rows, :] += jnp.dot(
                x_all[other, at, rows, :], buf_b[at].reshape(256, 640), preferred_element_type=F32
            )

    def wide_round(hop, _):
        for j in range(8):
            for g in wide:
                g.hop(hop, j)
            if (j // 2) % 2 == 0:
                wide_piece(j, hop - 1)
            else:
                @pl.when(hop > 1)
                def _():
                    wide_piece(j, hop - 1)
        return 0

    lax.fori_loop(1, 3, wide_round, 0)
    for j in range(8):
        for g in wide:
            g.hop(3, j)
        for g in deep:
            for i in (0, 1):
                g.send(MINUS if j < 4 else PLUS, 2 * (j % 4) + i)
        wide_piece(j, 2)
    for j in range(8):
        wide_piece(j, 3)
        for g in wide:
            g.last(j)
    for j, p in enumerate((0, 1, 4, 5)):
        wide_piece(p, 4)
        for g in deep:
            g.hop(1, 2 * j)
            g.hop(1, 2 * j + 1)

    def activate(k, _):
        rows = pl.ds(pl.multiple_of(k * 128, 128), 128)
        gate_at, up_at = (
            jnp.concatenate([v[...].reshape(1, 704), jnp.ones((1, 64), F32)], axis=1) for v in (gate_s, up_s)
        )
        left, right = acc_a[rows, :], acc_b[rows, :]
        tail = right[:, 512:640]
        g = jnp.concatenate([left[:, 0:640], tail], axis=1) * gate_at
        u = jnp.concatenate([left[:, 640:768], right[:, 0:512], pltpu.roll(tail, 64, 1)], axis=1) * up_at
        h = g / (1.0 + jnp.exp(-g)) * u
        lane = lax.broadcasted_iota(jnp.int32, h.shape, 1)
        h = jnp.where(lane < 704, h, 0.0)
        hid[k] = h.T.astype(BF16)
        return 0

    lax.fori_loop(0, 6, activate, 0)

    def half_of(which):
        return jnp.concatenate([hid[which * 3 + k] for k in range(3)], axis=1)

    def pair(group, at):
        give, got, sem = (give_a, got_a, pair_a) if group == 0 else (give_b, got_b, pair_b)
        return pltpu.make_async_remote_copy(
            src_ref=give.at[at], dst_ref=got.at[at], send_sem=pair_send.at[group], recv_sem=sem.at[at],
            device_id={"tp": peer}, device_id_type=MESH,
        )

    def deep_piece(p, away):
        block, mine = p % 4, p // 4
        sign = 1 if block % 2 == 0 else -1
        group = block // 2
        at = wrap((z, y)[group] + sign * away)
        left = (buf_c, buf_d)[group][at].reshape(128, 768)
        part = jnp.dot(left, half_of(core if mine else other), preferred_element_type=F32)
        if mine:
            (own_a, own_b)[group][at] = part
        else:
            (give_a, give_b)[group][at] = part.astype(BF16)
            pair(group, at).start()

    def put(group, src, slot, row, owner):
        dst, sem = (all_a.at[slot, core], x_a_sem) if group == 0 else (all_b.at[slot, core, row], x_b_sem)
        return pltpu.make_async_remote_copy(
            src_ref=src, dst_ref=dst, send_sem=x_send.at[group], recv_sem=sem.at[slot, core],
            device_id=(z, y, owner), device_id_type=MESH,
        )

    def relay(group, src, at):
        dst, sem = ((via_a, via_a_sem), (via_b, via_b_sem))[group]
        return pltpu.make_async_remote_copy(
            src_ref=src, dst_ref=dst.at[at], send_sem=x_send.at[group], recv_sem=sem.at[at],
            device_id=(z, y, place(onward, core)), device_id_type=MESH,
        )

    straight_slot = 1 + other
    added_slot = 1 + core

    def combine(group, at):
        pair(group, at).wait_recv()
        if group == 0:
            total = own_a[at] + got_a[at].astype(F32)
            low = total.astype(BF16).reshape(8, 16, 384)
            step = lax.rem(at // 2 - chip + 4, 4)

            @pl.when(at == tp)
            def _():
                all_a[0, core] = low

            @pl.when(at == peer)
            def _():
                sum_a[at] = low
                put(0, sum_a.at[at], 0, 0, at).start()

            @pl.when(step == 2)
            def _():
                sum_a[at] = low
                relay(0, sum_a.at[at], at).start()

            @pl.when(step == 2 + onward)
            def _():
                sum_a[at] = low
                put(0, sum_a.at[at], straight_slot, 0, at).start()

            @pl.when(step == 2 - onward)
            def _():
                own_a[at] = total
        else:
            total = own_b[at] + got_b[at].astype(F32)
            own_b[at] = total
            sum_b[at] = total.astype(BF16).reshape(8, 16, 384)
            relay(1, sum_b.at[at, pl.ds(place(2, 0), 2)], at).start()
            for c in (0, 1):
                owner = place(-onward, c)
                put(1, sum_b.at[at, owner], straight_slot, at, owner).start()
            put(1, sum_b.at[at, peer], 0, at, peer).start()
            all_b[0, core, at] = sum_b[at, tp]

    def finish(group, at):
        if group == 0:
            @pl.when(lax.rem(at // 2 - chip + 4, 4) == 2 - onward)
            def _():
                relay(0, sum_a.at[at], at).wait_recv()
                sum_a[at] = (own_a[at] + via_a[at].reshape(128, 384).astype(F32)).astype(BF16).reshape(8, 16, 384)
                put(0, sum_a.at[at], added_slot, 0, at).start()
        else:
            first = place(onward, 0)
            relay(1, sum_b.at[at, pl.ds(0, 2)], at).wait_recv()
            rows = pl.ds(pl.multiple_of(first * 16, 32), 32)
            total = own_b[at, rows, :] + via_b[at].reshape(32, 384).astype(F32)
            sum_b[at, pl.ds(first, 2)] = total.astype(BF16).reshape(2, 16, 384)
            for c in (0, 1):
                put(1, sum_b.at[at, first + c], added_slot, at, first + c).start()

    def each(act, away):
        for group, me in ((1, y), (0, z)):
            act(group, wrap(me + away))
            if 0 < away < 4:
                act(group, wrap(me - away))

    for j in range(8):
        for g in deep:
            g.hop(2, j)
        if j < 4:
            deep_piece((0, 2, 4, 6)[j], 0)
        deep_piece(j, 1)
        if j == 6:
            each(combine, 0)
    each(combine, 1)
    for j in range(8):
        for g in deep:
            g.hop(3, j)
        deep_piece(j, 2)
        if j == 3:
            each(finish, 0)
    each(combine, 2)
    each(finish, 1)
    for j in range(8):
        for g in deep:
            g.last(j)
        deep_piece(j, 3)
    each(combine, 3)
    each(finish, 2)
    for j in (0, 2, 4, 6):
        deep_piece(j, 4)
    each(combine, 4)
    each(finish, 3)
    each(finish, 4)

    for slot in range(3):
        for c in range(2):
            for ref, sem in ((all_a, x_a_sem), (all_b, x_b_sem)):
                landed = pltpu.make_async_copy(ref.at[slot, c], ref.at[slot, c], sem.at[slot, c])
                if slot:
                    landed.wait()
                else:
                    pl.when(core != c)(landed.wait)

    for h, held in ((0, all_a), (1, all_b)):
        for c in range(2):
            total = held[0, c].astype(F32) + held[1, c].astype(F32) + held[2, c].astype(F32)
            flat[:, h, :, c * 384 : c * 384 + 384] = total
    scale = down_s[...]
    for k in range(6):
        lanes = slice(k * 128, k * 128 + 128)
        block = flat[:, :, :, lanes].reshape(256, 128)
        out[lanes, :] = (block.T * scale).astype(BF16)

    for g in wide + deep:
        g.drain()
    for group, ref in ((0, give_a), (1, give_b)):
        pltpu.make_async_copy(ref, ref, pair_send.at[group]).wait()
    few = sum_a.at[pl.ds(0, 7)]
    pltpu.make_async_copy(few, few, x_send.at[0]).wait()
    few = sum_b.at[:, pl.ds(0, 7)]
    pltpu.make_async_copy(few, few, x_send.at[1]).wait()


def body(tokens, norm_gain, gate_weight, up_weight, gate_scale, up_scale, down_weight, down_scale):
    vmem = pl.BlockSpec(memory_space=pltpu.VMEM)
    hbm = pl.BlockSpec(memory_space=pl.ANY)
    dma = pltpu.SemaphoreType.DMA
    return pl.pallas_call(
        kernel,
        out_shape=jax.ShapeDtypeStruct((768, 256), BF16),
        in_specs=[hbm, vmem, hbm, hbm, vmem, vmem, hbm, vmem],
        out_specs=vmem,
        scratch_shapes=[
            pltpu.VMEM((768, 2048), BF16),
            pltpu.VMEM((32, 704), F32),
            pltpu.VMEM((32, 704), F32),
            pltpu.VMEM((32, 704), F32),
            pltpu.VMEM((2, 8, 768, 256), BF16),
            pltpu.VMEM((8, 8, 32, 768), BF16),
            pltpu.VMEM((8, 8, 32, 640), BF16),
            pltpu.VMEM((8, 8, 16, 768), BF16),
            pltpu.VMEM((8, 8, 16, 768), BF16),
            pltpu.VMEM((768, 768), F32),
            pltpu.VMEM((768, 640), F32),
            pltpu.VMEM((6, 768, 128), BF16),
            pltpu.VMEM((8, 128, 384), F32),
            pltpu.VMEM((8, 128, 384), F32),
            pltpu.VMEM((8, 128, 384), BF16),
            pltpu.VMEM((8, 128, 384), BF16),
            pltpu.VMEM((8, 128, 384), BF16),
            pltpu.VMEM((8, 128, 384), BF16),
            pltpu.VMEM((8, 8, 16, 384), BF16),
            pltpu.VMEM((8, 8, 16, 384), BF16),
            pltpu.VMEM((8, 8, 16, 384), BF16),
            pltpu.VMEM((8, 2, 16, 384), BF16),
            pltpu.VMEM((3, 2, 8, 16, 384), BF16),
            pltpu.VMEM((3, 2, 8, 16, 384), BF16),
            pltpu.VMEM((8, 2, 16, 768), F32),
            dma((4,)),
            dma((4,)),
            dma((4,)),
            dma((4, 2, 4)),
            dma((4, 2, 4, 8)),
            dma((2,)),
            dma((8,)),
            dma((8,)),
            dma((8,)),
            dma((8,)),
            dma((2,)),
            dma((3, 2)),
            dma((3, 2)),
        ],
        compiler_params=pltpu.CompilerParams(
            collective_id=0, has_side_effects=True, vmem_limit_bytes=56 * 1024 * 1024
        ),
    )(
        tokens, norm_gain.reshape(1, 2048), gate_weight, up_weight, gate_scale, up_scale,
        down_weight.T, down_scale.reshape(1, 256),
    )


def solution(mesh):
    split = Mesh(mesh.devices.reshape(8, 8, mesh.shape["tp"]), ("fs_0", "fs_1", "tp"))
    placed = (P(FS, None), P(), P(FS, "tp"), P(FS, "tp"), P("tp"), P("tp"), P("tp", FS), P("tp"))
    return jax.shard_map(body, mesh=split, in_specs=placed, out_specs=P(FS, "tp"), check_vma=False)
```

time: 95.9 us -> 87 us (0.907)
  the two profiles are of different devices: /device:TPU:5 before, /device:TPU:4 now
where the time goes in v2:
time: 87 us; the launch traced here: 86.8 us
  Pallas kernels  85 us (98%)
  local copies, waits for them, and re-layouts  1.77 us (2%)
    pallas_call x1, Pallas kernels, body(): pl.pallas_call(kernel, out_shape=jax.ShapeDtypeStruct((768, 256), BF16),...  85 us
    unnamed x1, local copies, waits for them, and re-layouts  1.77 us

profile of v2, /device:TPU:4, one launch (start us, length us, event | category | flops | bytes accessed | tf_op | source)
XLA Modules:
  0.0 86.8 jit_solution(3439940090471146083)
XLA Ops:
  0.0 85.0 %shard_map.82 = bf16[768,256]{1,0:T(8,128)(2,1)} custom-call(bf16[768,2048]{1,0:T(8,128)(2,1)} %tokens.1, f32[1,2048]{1,0:T(1,128)} %bitcast.4, f32[32,704]{1,0:T(8,128)} %gate_w.1, f32[32,704]{1,0:T(8,128)} %up_w.1, f32[704]{0:T(1024)} %gate_s.1, f32[704]{0:T(1024)} %up_s.1, f32[32,704]{1,0:T(8,128)} %bitcast.3, f32[1,256]{1,0:T(1,128)} %bitcast.5), custom_call_target="tpu_custom_call" | custom-call | tf_op jit(solution)/shard_map/pallas_call | solution.py:402
  85.0 1.8 %copy.10 = bf16[768,256]{1,0:T(8,128)(2,1)} copy(bf16[768,256]{1,0:T(8,128)(2,1)} %shard_map.82) | data formatting | bytes 786432

commit v3 on v2

--- a/solution.py
+++ b/solution.py
@@ -11,6 +11,7 @@
 F32, BF16 = jnp.float32, jnp.bfloat16
 OFF = (0, 1, -1, 2, -2, 3, -3, 4)
 PLUS, MINUS = 0, 1
+LATE = 4
 
 
 def wrap(i):
@@ -32,8 +33,11 @@
 
     def second(self, way, hop, j, source):
         at = self.buf.at[wrap(self.major + source), wrap(self.minor + OFF[j])]
+        if hop == 4:
+            half = self.buf.shape[2] // 2
+            at = at.at[pl.ds(way * half, half)]
         return pltpu.make_async_remote_copy(
-            src_ref=at, dst_ref=at, send_sem=self.send2, recv_sem=self.recv2.at[way, hop - 1, j],
+            src_ref=at, dst_ref=at, send_sem=self.send2, recv_sem=self.recv2.at[self.number(way, hop, j // 2)],
             device_id=self.along_major[way], device_id_type=MESH,
         )
 
@@ -41,12 +45,15 @@
         self.first(PLUS, 1, 0).start()
         self.first(MINUS, 1, 0).start()
 
-    def start_second(self, j):
-        self.send(PLUS, j)
-        self.send(MINUS, j)
-
     def send(self, way, j):
         self.second(way, 1, j, 0).start()
+
+    def number(self, way, hop, pair):
+        return 8 * (hop - 1) + 4 * way + pair
+
+    def arrive(self, way, hop, pair):
+        here = self.buf.at[0, pl.ds(0, 2 if hop < 4 else 1)]
+        pltpu.make_async_copy(here, here, self.recv2.at[self.number(way, hop, pair)]).wait()
 
     def line(self, step):
         self.first(PLUS, step, -step).wait_recv()
@@ -56,17 +63,12 @@
         if step < 3:
             self.first(MINUS, step + 1, step).start()
 
-    def hop(self, hop, j):
-        for way, side, last in ((PLUS, -1, j < 4), (MINUS, 1, j >= 4)):
-            self.second(way, hop, j, side * hop).wait_recv()
-            if last or not isinstance(hop, int) or hop < 3:
-                self.second(way, hop + 1, j, side * hop).start()
-
-    def last(self, j):
-        if j < 4:
-            self.second(PLUS, 4, j, -4).wait_recv()
-        else:
-            self.second(MINUS, 4, j, 4).wait_recv()
+    def hop(self, hop, pair):
+        for way, side in ((PLUS, -1), (MINUS, 1)):
+            self.arrive(way, hop, pair)
+            if hop < 4:
+                for j in (2 * pair, 2 * pair + 1):
+                    self.second(way, hop + 1, j, side * hop).start()
 
     def drain(self):
         one = self.buf.at[0, pl.ds(0, 7)]
@@ -77,7 +79,7 @@
 
 def kernel(
     tokens, gain, gate_w, up_w, gate_s, up_s, down_w, down_s, out,
-    tok, gw_in, uw_in, dw_in, x_all, buf_a, buf_b, buf_c, buf_d, acc_a, acc_b, hid,
+    tok, gw_in, uw_in, dw_in, gain_in, gs_in, us_in, ds_in, perm, x_all, buf_a, buf_b, buf_c, buf_d, acc_a, acc_b, hid,
     own_a, own_b, give_a, give_b, got_a, got_b, sum_a, sum_b, via_a, via_b, all_a, all_b, flat,
     in_sem, send1, send2, recv1, recv2, pair_send, pair_a, pair_b, via_a_sem, via_b_sem, x_send, x_a_sem, x_b_sem,
 ):
@@ -93,14 +95,20 @@
 
     along_z = [(wrap(z + side), y, tp) for side in (1, -1)]
     along_y = [(z, wrap(y + side), tp) for side in (1, -1)]
+    all_a[3] = jnp.zeros((2, 8, 16, 384), BF16)
+    all_b[3] = jnp.zeros((2, 8, 16, 384), BF16)
+
     barrier = pltpu.get_barrier_semaphore()
-    near = along_z + along_y + [(z, y, peer)] + [(z, y, place(step, c)) for step in (1, 3) for c in (0, 1)]
+    near = along_z + along_y + [(z, y, lax.rem(tp + k, 8)) for k in range(1, 8)]
     for device in near:
         pl.semaphore_signal(barrier, inc=1, device_id=device, device_id_type=MESH)
 
+    inputs = (
+        (gate_w, gw_in), (up_w, uw_in), (down_w, dw_in), (tokens, tok), (gain, gain_in), (gate_s, gs_in), (up_s, us_in), (down_s, ds_in),
+    )
     fetches = [
         pltpu.make_async_copy(src, dst, in_sem.at[k])
-        for k, (src, dst) in enumerate(((gate_w, gw_in), (up_w, uw_in), (down_w, dw_in), (tokens, tok)))
+        for k, (src, dst) in enumerate(inputs)
     ]
     for fetch in fetches:
         fetch.start()
@@ -129,49 +137,74 @@
     buf_a[major, minor, :, 640:768] = uw[:, 0:128]
     buf_b[minor, major, :, 0:512] = uw[:, 128:640]
     buf_b[minor, major, :, 512:640] = jnp.concatenate([gw[:, 640:], uw[:, 640:]], axis=1)
+    pl.semaphore_wait(barrier, len(near))
+    for g in wide:
+        g.start_first()
+    for g in wide:
+        for way in (PLUS, MINUS):
+            g.send(way, 0)
     fetches[2].wait()
     turned = jnp.concatenate([dw_in[...], jnp.zeros((32, 64), F32)], axis=1).astype(BF16)
     buf_c[z, y] = turned[0:16]
     buf_d[y, z] = turned[16:32]
-
-    pl.semaphore_wait(barrier, len(near))
-    for g in wide + deep:
+    for g in deep:
         g.start_first()
-    for g in wide:
-        g.start_second(0)
-
-    acc_a[...] = jnp.zeros_like(acc_a)
-    acc_b[...] = jnp.zeros_like(acc_b)
-    fetches[3].wait()
-
-    def prepare(k, _):
-        rows = pl.ds(pl.multiple_of(k * 16, 16), 16)
-        values = tok[rows, :].astype(F32)
-        normed = values * lax.rsqrt(jnp.mean(values * values, axis=-1, keepdims=True) + 1e-06) * gain[...]
-        for b in range(8):
-            x_all[0, b, rows, :] = normed[:, b * 256 : b * 256 + 256].astype(BF16)
-        lane = lax.broadcasted_iota(jnp.int32, (16, 128), 1) // 32
-        for yy in range(8):
-            for zh in range(2):
-                tile = None
-                for zl in range(4):
-                    t = (zh * 4 + zl) * 2 + yy // 4
-                    piece = normed[:, t * 128 : t * 128 + 128]
-                    shift = ((zl - yy % 4) * 32) % 128
-                    if shift:
-                        piece = pltpu.roll(piece, shift, 1)
-                    tile = piece if tile is None else jnp.where(lane == zl, piece, tile)
-                x_all[1, yy, rows, zh * 128 : zh * 128 + 128] = tile.astype(BF16)
+
+    for fetch in fetches[3:]:
+        fetch.wait()
+
+    def normalize(k, _):
+        rows = pl.ds(pl.multiple_of(k * 64, 64), 64)
+        squares = jnp.zeros((64, 128), F32)
+        for t in range(16):
+            v = tok[rows, t * 128 : t * 128 + 128].astype(F32)
+            squares += v * v
+        factor = lax.rsqrt(jnp.sum(squares, axis=-1, keepdims=True) * (1 / 2048) + 1e-06)
+        for t in range(16):
+            v = tok[rows, t * 128 : t * 128 + 128].astype(F32) * factor * gain_in[:, t * 128 : t * 128 + 128]
+            x_all[0, t // 2, rows, t % 2 * 128 : t % 2 * 128 + 128] = v.astype(BF16)
         return 0
+
+    lax.fori_loop(0, 5, normalize, 0)
+
+    k, n = (lax.broadcasted_iota(jnp.int32, (512, 512), d) for d in (0, 1))
+    chosen = (k // 128 == n % 128 // 32) & (k % 128 // 32 == n // 128) & (k % 32 == n % 32)
+    perm[...] = chosen.astype(F32).astype(BF16)
+
+    def permute(group):
+        zh, yh = group // 2, group % 2
+
+        def some(k, _):
+            rows = pl.ds(pl.multiple_of(k * 256, 256), 256)
+            source = jnp.concatenate([x_all[0, zh * 4 + zl, rows, yh * 128 : yh * 128 + 128] for zl in range(4)], axis=1)
+            moved = jnp.dot(source, perm[...], preferred_element_type=F32).astype(BF16)
+            for yq in range(4):
+                x_all[1, yh * 4 + yq, rows, zh * 128 : zh * 128 + 128] = moved[:, yq * 128 : yq * 128 + 128]
+            return 0
+
+        lax.fori_loop(0, 3, some, 0)
 
     for step in range(1, 5):
         for g in wide + deep:
             g.line(step)
-        for g in wide:
-            g.start_second(2 * step - 1)
-            if step < 4:
-                g.start_second(2 * step)
-        lax.fori_loop((step - 1) * 12, step * 12, prepare, 0)
+        for j in (2 * step - 1, 2 * step):
+            for g in wide:
+                for way in (PLUS, MINUS):
+                    if j < 8:
+                        g.send(way, j)
+        if step < 4:
+            lax.fori_loop((5, 8, 10)[step - 1], (8, 10, 12)[step - 1], normalize, 0)
+        if step > 1:
+            for g in wide:
+                g.hop(1, step - 2)
+    permute(0)
+    permute(1)
+    for g in wide:
+        g.hop(1, 3)
+    permute(2)
+    permute(3)
+    acc_a[...] = jnp.zeros_like(acc_a)
+    acc_b[...] = jnp.zeros_like(acc_b)
 
     def wide_piece(p, away):
         block, half = p // 2, p % 2
@@ -188,40 +221,39 @@
                 x_all[other, at, rows, :], buf_b[at].reshape(256, 640), preferred_element_type=F32
             )
 
-    def wide_round(hop, _):
-        for j in range(8):
-            for g in wide:
-                g.hop(hop, j)
-            if (j // 2) % 2 == 0:
-                wide_piece(j, hop - 1)
-            else:
-                @pl.when(hop > 1)
-                def _():
-                    wide_piece(j, hop - 1)
-        return 0
-
-    lax.fori_loop(1, 3, wide_round, 0)
+    for pair in range(4):
+        for g in wide:
+            g.hop(2, pair)
+        wide_piece((0, 1, 4, 5)[pair], 0)
+        wide_piece(2 * pair, 1)
+        wide_piece(2 * pair + 1, 1)
+    for pair in range(4):
+        for g in wide:
+            g.hop(3, pair)
+        wide_piece(2 * pair, 2)
+        wide_piece(2 * pair + 1, 2)
     for j in range(8):
+        for g in deep:
+            for way in (PLUS, MINUS):
+                g.send(way, j)
+    for pair in range(4):
+        wide_piece(2 * pair, 3)
+        wide_piece(2 * pair + 1, 3)
         for g in wide:
-            g.hop(3, j)
+            g.hop(4, pair)
+    for p in (0, 1, 4, 5):
+        wide_piece(p, 4)
+
+    def deep_hop(hop, pair):
         for g in deep:
-            for i in (0, 1):
-                g.send(MINUS if j < 4 else PLUS, 2 * (j % 4) + i)
-        wide_piece(j, 2)
-    for j in range(8):
-        wide_piece(j, 3)
-        for g in wide:
-            g.last(j)
-    for j, p in enumerate((0, 1, 4, 5)):
-        wide_piece(p, 4)
-        for g in deep:
-            g.hop(1, 2 * j)
-            g.hop(1, 2 * j + 1)
+            g.hop(hop, pair)
+
+    deep_hop(1, 0)
 
     def activate(k, _):
         rows = pl.ds(pl.multiple_of(k * 128, 128), 128)
         gate_at, up_at = (
-            jnp.concatenate([v[...].reshape(1, 704), jnp.ones((1, 64), F32)], axis=1) for v in (gate_s, up_s)
+            jnp.concatenate([v[...].reshape(1, 704), jnp.ones((1, 64), F32)], axis=1) for v in (gs_in, us_in)
         )
         left, right = acc_a[rows, :], acc_b[rows, :]
         tail = right[:, 512:640]
@@ -238,7 +270,7 @@
     def half_of(which):
         return jnp.concatenate([hid[which * 3 + k] for k in range(3)], axis=1)
 
-    def pair(group, at):
+    def exchange(group, at):
         give, got, sem = (give_a, got_a, pair_a) if group == 0 else (give_b, got_b, pair_b)
         return pltpu.make_async_remote_copy(
             src_ref=give.at[at], dst_ref=got.at[at], send_sem=pair_send.at[group], recv_sem=sem.at[at],
@@ -256,7 +288,7 @@
             (own_a, own_b)[group][at] = part
         else:
             (give_a, give_b)[group][at] = part.astype(BF16)
-            pair(group, at).start()
+            exchange(group, at).start()
 
     def put(group, src, slot, row, owner):
         dst, sem = (all_a.at[slot, core], x_a_sem) if group == 0 else (all_b.at[slot, core, row], x_b_sem)
@@ -275,8 +307,8 @@
     straight_slot = 1 + other
     added_slot = 1 + core
 
-    def combine(group, at):
-        pair(group, at).wait_recv()
+    def combine_one(group, at, late):
+        exchange(group, at).wait_recv()
         if group == 0:
             total = own_a[at] + got_a[at].astype(F32)
             low = total.astype(BF16).reshape(8, 16, 384)
@@ -286,36 +318,45 @@
             def _():
                 all_a[0, core] = low
 
+            @pl.when(at != tp)
+            def _():
+                sum_a[at] = low
+
             @pl.when(at == peer)
             def _():
-                sum_a[at] = low
                 put(0, sum_a.at[at], 0, 0, at).start()
 
             @pl.when(step == 2)
             def _():
-                sum_a[at] = low
-                relay(0, sum_a.at[at], at).start()
+                (put(0, sum_a.at[at], 3, 0, at) if late else relay(0, sum_a.at[at], at)).start()
 
             @pl.when(step == 2 + onward)
             def _():
-                sum_a[at] = low
                 put(0, sum_a.at[at], straight_slot, 0, at).start()
 
             @pl.when(step == 2 - onward)
             def _():
-                own_a[at] = total
+                if late:
+                    put(0, sum_a.at[at], added_slot, 0, at).start()
+                else:
+                    own_a[at] = total
         else:
             total = own_b[at] + got_b[at].astype(F32)
-            own_b[at] = total
             sum_b[at] = total.astype(BF16).reshape(8, 16, 384)
-            relay(1, sum_b.at[at, pl.ds(place(2, 0), 2)], at).start()
+            if late:
+                for c in (0, 1):
+                    put(1, sum_b.at[at, place(2, c)], 3, at, place(2, c)).start()
+                for c in (0, 1):
+                    put(1, sum_b.at[at, place(onward, c)], added_slot, at, place(onward, c)).start()
+            else:
+                own_b[at] = total
+                relay(1, sum_b.at[at, pl.ds(place(2, 0), 2)], at).start()
             for c in (0, 1):
-                owner = place(-onward, c)
-                put(1, sum_b.at[at, owner], straight_slot, at, owner).start()
+                put(1, sum_b.at[at, place(-onward, c)], straight_slot, at, place(-onward, c)).start()
             put(1, sum_b.at[at, peer], 0, at, peer).start()
             all_b[0, core, at] = sum_b[at, tp]
 
-    def finish(group, at):
+    def finish_one(group, at):
         if group == 0:
             @pl.when(lax.rem(at // 2 - chip + 4, 4) == 2 - onward)
             def _():
@@ -331,55 +372,77 @@
             for c in (0, 1):
                 put(1, sum_b.at[at, first + c], added_slot, at, first + c).start()
 
-    def each(act, away):
-        for group, me in ((1, y), (0, z)):
+    def both_sides(act, away):
+        for group, me in ((0, z), (1, y)):
             act(group, wrap(me + away))
             if 0 < away < 4:
                 act(group, wrap(me - away))
 
-    for j in range(8):
-        for g in deep:
-            g.hop(2, j)
-        if j < 4:
-            deep_piece((0, 2, 4, 6)[j], 0)
-        deep_piece(j, 1)
-        if j == 6:
-            each(combine, 0)
-    each(combine, 1)
-    for j in range(8):
-        for g in deep:
-            g.hop(3, j)
-        deep_piece(j, 2)
-        if j == 3:
-            each(finish, 0)
-    each(combine, 2)
-    each(finish, 1)
-    for j in range(8):
-        for g in deep:
-            g.last(j)
-        deep_piece(j, 3)
-    each(combine, 3)
-    each(finish, 2)
-    for j in (0, 2, 4, 6):
-        deep_piece(j, 4)
-    each(combine, 4)
-    each(finish, 3)
-    each(finish, 4)
-
-    for slot in range(3):
-        for c in range(2):
-            for ref, sem in ((all_a, x_a_sem), (all_b, x_b_sem)):
-                landed = pltpu.make_async_copy(ref.at[slot, c], ref.at[slot, c], sem.at[slot, c])
-                if slot:
-                    landed.wait()
+    def combine(away):
+        both_sides(lambda group, at: combine_one(group, at, away >= LATE), away)
+
+    def finish(away):
+        both_sides(finish_one, away)
+
+    def deep_pieces(which, away):
+        for p in which:
+            deep_piece(p, away)
+
+    deep_hop(1, 1)
+    deep_pieces((0, 2, 4, 6), 0)
+    deep_hop(1, 2)
+    combine(0)
+    deep_hop(1, 3)
+    deep_pieces((0, 1, 2, 3), 1)
+    deep_hop(2, 0)
+    deep_pieces((4, 5), 1)
+    deep_hop(2, 1)
+    deep_pieces((6, 7), 1)
+    combine(1)
+    deep_hop(2, 2)
+    deep_hop(2, 3)
+    finish(0)
+    deep_pieces((0, 1, 2, 3), 2)
+    deep_hop(3, 0)
+    deep_pieces((4, 5, 6, 7), 2)
+    deep_hop(3, 1)
+    combine(2)
+    deep_hop(3, 2)
+    deep_hop(3, 3)
+    finish(1)
+    deep_pieces((0, 1, 2, 3, 4, 5, 6, 7), 3)
+    combine(3)
+    finish(2)
+    for pair in range(4):
+        deep_hop(4, pair)
+    deep_pieces((0, 2, 4, 6), 4)
+    combine(4)
+    finish(3)
+
+    apart = lax.rem(tp - z + 8, 8)
+    far_a = (apart >= LATE) & (apart <= 8 - LATE)
+    for c in range(2):
+        for slot in range(4):
+            rows = pl.ds(0, 8 if slot < 3 else 9 - 2 * LATE)
+            wait_a = pltpu.make_async_copy(all_a.at[slot, c], all_a.at[slot, c], x_a_sem.at[slot, c]).wait
+            wait_b = pltpu.make_async_copy(all_b.at[slot, c, rows], all_b.at[slot, c, rows], x_b_sem.at[slot, c]).wait
+            if slot == 0:
+                pl.when(core != c)(wait_a)
+                pl.when(core != c)(wait_b)
+            else:
+                if slot < 3:
+                    wait_a()
                 else:
-                    pl.when(core != c)(landed.wait)
+                    pl.when(far_a)(wait_a)
+                wait_b()
 
     for h, held in ((0, all_a), (1, all_b)):
         for c in range(2):
-            total = held[0, c].astype(F32) + held[1, c].astype(F32) + held[2, c].astype(F32)
+            total = held[0, c].astype(F32)
+            for slot in range(1, 4):
+                total += held[slot, c].astype(F32)
             flat[:, h, :, c * 384 : c * 384 + 384] = total
-    scale = down_s[...]
+    scale = ds_in[...]
     for k in range(6):
         lanes = slice(k * 128, k * 128 + 128)
         block = flat[:, :, :, lanes].reshape(256, 128)
@@ -402,13 +465,18 @@
     return pl.pallas_call(
         kernel,
         out_shape=jax.ShapeDtypeStruct((768, 256), BF16),
-        in_specs=[hbm, vmem, hbm, hbm, vmem, vmem, hbm, vmem],
+        in_specs=[hbm] * 8,
         out_specs=vmem,
         scratch_shapes=[
             pltpu.VMEM((768, 2048), BF16),
             pltpu.VMEM((32, 704), F32),
             pltpu.VMEM((32, 704), F32),
             pltpu.VMEM((32, 704), F32),
+            pltpu.VMEM((1, 2048), F32),
+            pltpu.VMEM((704,), F32),
+            pltpu.VMEM((704,), F32),
+            pltpu.VMEM((1, 256), F32),
+            pltpu.VMEM((512, 512), BF16),
             pltpu.VMEM((2, 8, 768, 256), BF16),
             pltpu.VMEM((8, 8, 32, 768), BF16),
             pltpu.VMEM((8, 8, 32, 640), BF16),
@@ -427,22 +495,22 @@
             pltpu.VMEM((8, 8, 16, 384), BF16),
             pltpu.VMEM((8, 8, 16, 384), BF16),
             pltpu.VMEM((8, 2, 16, 384), BF16),
-            pltpu.VMEM((3, 2, 8, 16, 384), BF16),
-            pltpu.VMEM((3, 2, 8, 16, 384), BF16),
+            pltpu.VMEM((4, 2, 8, 16, 384), BF16),
+            pltpu.VMEM((4, 2, 8, 16, 384), BF16),
             pltpu.VMEM((8, 2, 16, 768), F32),
-            dma((4,)),
+            dma((8,)),
             dma((4,)),
             dma((4,)),
             dma((4, 2, 4)),
-            dma((4, 2, 4, 8)),
+            dma((4, 32)),
             dma((2,)),
             dma((8,)),
             dma((8,)),
             dma((8,)),
             dma((8,)),
             dma((2,)),
-            dma((3, 2)),
-            dma((3, 2)),
+            dma((4, 2)),
+            dma((4, 2)),
         ],
         compiler_params=pltpu.CompilerParams(
             collective_id=0, has_side_effects=True, vmem_limit_bytes=56 * 1024 * 1024

time: 87 us -> 82.9 us (0.953)
  the two profiles are of different devices: /device:TPU:4 before, /device:TPU:3 now
where the time goes in v3:
time: 82.9 us; the launch traced here: 82.8 us
  Pallas kernels  81 us (98%)
  local copies, waits for them, and re-layouts  1.77 us (2%)
    pallas_call x1, Pallas kernels, body(): pl.pallas_call(kernel, out_shape=jax.ShapeDtypeStruct((768, 256), BF16),...  81 us
    unnamed x1, local copies, waits for them, and re-layouts  1.77 us

profile of v3, /device:TPU:3, one launch (start us, length us, event | category | flops | bytes accessed | tf_op | source)
XLA Modules:
  0.0 82.8 jit_solution(1127409136388225537)
XLA Ops:
  0.0 81.0 %shard_map.82 = bf16[768,256]{1,0:T(8,128)(2,1)} custom-call(bf16[768,2048]{1,0:T(8,128)(2,1)} %tokens.1, f32[1,2048]{1,0:T(1,128)} %bitcast.4, f32[32,704]{1,0:T(8,128)} %gate_w.1, f32[32,704]{1,0:T(8,128)} %up_w.1, f32[704]{0:T(1024)} %gate_s.1, f32[704]{0:T(1024)} %up_s.1, f32[32,704]{1,0:T(8,128)} %bitcast.3, f32[1,256]{1,0:T(1,128)} %bitcast.5), custom_call_target="tpu_custom_call" | custom-call | tf_op jit(solution)/shard_map/pallas_call | solution.py:465
  81.0 1.8 %copy.10 = bf16[768,256]{1,0:T(8,128)(2,1)} copy(bf16[768,256]{1,0:T(8,128)(2,1)} %shard_map.82) | data formatting | bytes 786432

commit v4 on v3

--- a/solution.py
+++ b/solution.py
@@ -11,7 +11,7 @@
 F32, BF16 = jnp.float32, jnp.bfloat16
 OFF = (0, 1, -1, 2, -2, 3, -3, 4)
 PLUS, MINUS = 0, 1
-LATE = 4
+WIDE, DEEP = (2, 4, 4, 4), (2, 2, 2, 8)
 
 
 def wrap(i):
@@ -19,8 +19,8 @@
 
 
 class Gather:
-    def __init__(self, buf, major, minor, along_major, along_minor, sems):
-        self.buf, self.major, self.minor = buf, major, minor
+    def __init__(self, buf, major, minor, along_major, along_minor, sems, sizes):
+        self.buf, self.major, self.minor, self.sizes = buf, major, minor, sizes
         self.along_major, self.along_minor = along_major, along_minor
         self.send1, self.send2, self.recv1, self.recv2 = sems
 
@@ -37,7 +37,7 @@
             half = self.buf.shape[2] // 2
             at = at.at[pl.ds(way * half, half)]
         return pltpu.make_async_remote_copy(
-            src_ref=at, dst_ref=at, send_sem=self.send2, recv_sem=self.recv2.at[self.number(way, hop, j // 2)],
+            src_ref=at, dst_ref=at, send_sem=self.send2, recv_sem=self.recv2.at[self.number(way, hop, j // self.sizes[hop - 1])],
             device_id=self.along_major[way], device_id_type=MESH,
         )
 
@@ -48,12 +48,14 @@
     def send(self, way, j):
         self.second(way, 1, j, 0).start()
 
-    def number(self, way, hop, pair):
-        return 8 * (hop - 1) + 4 * way + pair
-
-    def arrive(self, way, hop, pair):
-        here = self.buf.at[0, pl.ds(0, 2 if hop < 4 else 1)]
-        pltpu.make_async_copy(here, here, self.recv2.at[self.number(way, hop, pair)]).wait()
+    def number(self, way, hop, group):
+        counts = [8 // size for size in self.sizes]
+        return 2 * sum(counts[: hop - 1]) + way * counts[hop - 1] + group
+
+    def arrive(self, way, hop, group):
+        size = self.sizes[hop - 1]
+        here = self.buf.at[0, pl.ds(0, size if hop < 4 else size // 2)]
+        pltpu.make_async_copy(here, here, self.recv2.at[self.number(way, hop, group)]).wait()
 
     def line(self, step):
         self.first(PLUS, step, -step).wait_recv()
@@ -63,11 +65,12 @@
         if step < 3:
             self.first(MINUS, step + 1, step).start()
 
-    def hop(self, hop, pair):
+    def hop(self, hop, group):
+        size = self.sizes[hop - 1]
         for way, side in ((PLUS, -1), (MINUS, 1)):
-            self.arrive(way, hop, pair)
+            self.arrive(way, hop, group)
             if hop < 4:
-                for j in (2 * pair, 2 * pair + 1):
+                for j in range(group * size, group * size + size):
                     self.second(way, hop + 1, j, side * hop).start()
 
     def drain(self):
@@ -95,11 +98,8 @@
 
     along_z = [(wrap(z + side), y, tp) for side in (1, -1)]
     along_y = [(z, wrap(y + side), tp) for side in (1, -1)]
-    all_a[3] = jnp.zeros((2, 8, 16, 384), BF16)
-    all_b[3] = jnp.zeros((2, 8, 16, 384), BF16)
-
     barrier = pltpu.get_barrier_semaphore()
-    near = along_z + along_y + [(z, y, lax.rem(tp + k, 8)) for k in range(1, 8)]
+    near = along_z + along_y + [(z, y, peer)] + [(z, y, place(step, c)) for step in (1, 3) for c in (0, 1)]
     for device in near:
         pl.semaphore_signal(barrier, inc=1, device_id=device, device_id_type=MESH)
 
@@ -124,10 +124,10 @@
     def sems(k):
         return send1.at[k], send2.at[k], recv1.at[k], recv2.at[k]
 
-    ga = Gather(buf_a, major, minor, along_major, along_minor, sems(0))
-    gb = Gather(buf_b, minor, major, along_minor, along_major, sems(1))
-    gc = Gather(buf_c, z, y, along_z, along_y, sems(2))
-    gd = Gather(buf_d, y, z, along_y, along_z, sems(3))
+    ga = Gather(buf_a, major, minor, along_major, along_minor, sems(0), WIDE)
+    gb = Gather(buf_b, minor, major, along_minor, along_major, sems(1), WIDE)
+    gc = Gather(buf_c, z, y, along_z, along_y, sems(2), DEEP)
+    gd = Gather(buf_d, y, z, along_y, along_z, sems(3), DEEP)
     wide, deep = (ga, gb), (gc, gd)
 
     fetches[0].wait()
@@ -149,6 +149,9 @@
     buf_d[y, z] = turned[16:32]
     for g in deep:
         g.start_first()
+    for g in deep:
+        for way in (PLUS, MINUS):
+            g.send(way, 0)
 
     for fetch in fetches[3:]:
         fetch.wait()
@@ -185,13 +188,14 @@
         lax.fori_loop(0, 3, some, 0)
 
     for step in range(1, 5):
-        for g in wide + deep:
+        for g in wide:
             g.line(step)
-        for j in (2 * step - 1, 2 * step):
-            for g in wide:
+            for j in (2 * step - 1, 2 * step):
                 for way in (PLUS, MINUS):
                     if j < 8:
                         g.send(way, j)
+        for g in deep:
+            g.line(step)
         if step < 4:
             lax.fori_loop((5, 8, 10)[step - 1], (8, 10, 12)[step - 1], normalize, 0)
         if step > 1:
@@ -221,32 +225,33 @@
                 x_all[other, at, rows, :], buf_b[at].reshape(256, 640), preferred_element_type=F32
             )
 
-    for pair in range(4):
+    for group in range(2):
         for g in wide:
-            g.hop(2, pair)
-        wide_piece((0, 1, 4, 5)[pair], 0)
-        wide_piece(2 * pair, 1)
-        wide_piece(2 * pair + 1, 1)
-    for pair in range(4):
+            g.hop(2, group)
+        for p in (0, 1, 4, 5)[2 * group : 2 * group + 2]:
+            wide_piece(p, 0)
+        for p in range(4 * group, 4 * group + 4):
+            wide_piece(p, 1)
+    for group in range(2):
         for g in wide:
-            g.hop(3, pair)
-        wide_piece(2 * pair, 2)
-        wide_piece(2 * pair + 1, 2)
-    for j in range(8):
+            g.hop(3, group)
+        for p in range(4 * group, 4 * group + 4):
+            wide_piece(p, 2)
+    for j in range(1, 8):
         for g in deep:
             for way in (PLUS, MINUS):
                 g.send(way, j)
-    for pair in range(4):
-        wide_piece(2 * pair, 3)
-        wide_piece(2 * pair + 1, 3)
+    for group in range(2):
+        for p in range(4 * group, 4 * group + 4):
+            wide_piece(p, 3)
         for g in wide:
-            g.hop(4, pair)
+            g.hop(4, group)
     for p in (0, 1, 4, 5):
         wide_piece(p, 4)
 
-    def deep_hop(hop, pair):
+    def deep_hop(hop, group):
         for g in deep:
-            g.hop(hop, pair)
+            g.hop(hop, group)
 
     deep_hop(1, 0)
 
@@ -307,7 +312,7 @@
     straight_slot = 1 + other
     added_slot = 1 + core
 
-    def combine_one(group, at, late):
+    def combine_one(group, at):
         exchange(group, at).wait_recv()
         if group == 0:
             total = own_a[at] + got_a[at].astype(F32)
@@ -328,7 +333,7 @@
 
             @pl.when(step == 2)
             def _():
-                (put(0, sum_a.at[at], 3, 0, at) if late else relay(0, sum_a.at[at], at)).start()
+                relay(0, sum_a.at[at], at).start()
 
             @pl.when(step == 2 + onward)
             def _():
@@ -336,21 +341,12 @@
 
             @pl.when(step == 2 - onward)
             def _():
-                if late:
-                    put(0, sum_a.at[at], added_slot, 0, at).start()
-                else:
-                    own_a[at] = total
+                own_a[at] = total
         else:
             total = own_b[at] + got_b[at].astype(F32)
             sum_b[at] = total.astype(BF16).reshape(8, 16, 384)
-            if late:
-                for c in (0, 1):
-                    put(1, sum_b.at[at, place(2, c)], 3, at, place(2, c)).start()
-                for c in (0, 1):
-                    put(1, sum_b.at[at, place(onward, c)], added_slot, at, place(onward, c)).start()
-            else:
-                own_b[at] = total
-                relay(1, sum_b.at[at, pl.ds(place(2, 0), 2)], at).start()
+            own_b[at] = total
+            relay(1, sum_b.at[at, pl.ds(place(2, 0), 2)], at).start()
             for c in (0, 1):
                 put(1, sum_b.at[at, place(-onward, c)], straight_slot, at, place(-onward, c)).start()
             put(1, sum_b.at[at, peer], 0, at, peer).start()
@@ -379,7 +375,7 @@
                 act(group, wrap(me - away))
 
     def combine(away):
-        both_sides(lambda group, at: combine_one(group, at, away >= LATE), away)
+        both_sides(combine_one, away)
 
     def finish(away):
         both_sides(finish_one, away)
@@ -391,8 +387,8 @@
     deep_hop(1, 1)
     deep_pieces((0, 2, 4, 6), 0)
     deep_hop(1, 2)
+    deep_hop(1, 3)
     combine(0)
-    deep_hop(1, 3)
     deep_pieces((0, 1, 2, 3), 1)
     deep_hop(2, 0)
     deep_pieces((4, 5), 1)
@@ -413,33 +409,27 @@
     deep_pieces((0, 1, 2, 3, 4, 5, 6, 7), 3)
     combine(3)
     finish(2)
-    for pair in range(4):
-        deep_hop(4, pair)
+    deep_hop(4, 0)
     deep_pieces((0, 2, 4, 6), 4)
     combine(4)
     finish(3)
-
-    apart = lax.rem(tp - z + 8, 8)
-    far_a = (apart >= LATE) & (apart <= 8 - LATE)
+    finish(4)
+
     for c in range(2):
-        for slot in range(4):
-            rows = pl.ds(0, 8 if slot < 3 else 9 - 2 * LATE)
+        for slot in range(3):
             wait_a = pltpu.make_async_copy(all_a.at[slot, c], all_a.at[slot, c], x_a_sem.at[slot, c]).wait
-            wait_b = pltpu.make_async_copy(all_b.at[slot, c, rows], all_b.at[slot, c, rows], x_b_sem.at[slot, c]).wait
-            if slot == 0:
+            wait_b = pltpu.make_async_copy(all_b.at[slot, c], all_b.at[slot, c], x_b_sem.at[slot, c]).wait
+            if slot:
+                wait_a()
+                wait_b()
+            else:
                 pl.when(core != c)(wait_a)
                 pl.when(core != c)(wait_b)
-            else:
-                if slot < 3:
-                    wait_a()
-                else:
-                    pl.when(far_a)(wait_a)
-                wait_b()
 
     for h, held in ((0, all_a), (1, all_b)):
         for c in range(2):
             total = held[0, c].astype(F32)
-            for slot in range(1, 4):
+            for slot in range(1, 3):
                 total += held[slot, c].astype(F32)
             flat[:, h, :, c * 384 : c * 384 + 384] = total
     scale = ds_in[...]
@@ -495,22 +485,22 @@
             pltpu.VMEM((8, 8, 16, 384), BF16),
             pltpu.VMEM((8, 8, 16, 384), BF16),
             pltpu.VMEM((8, 2, 16, 384), BF16),
-            pltpu.VMEM((4, 2, 8, 16, 384), BF16),
-            pltpu.VMEM((4, 2, 8, 16, 384), BF16),
+            pltpu.VMEM((3, 2, 8, 16, 384), BF16),
+            pltpu.VMEM((3, 2, 8, 16, 384), BF16),
             pltpu.VMEM((8, 2, 16, 768), F32),
             dma((8,)),
             dma((4,)),
             dma((4,)),
             dma((4, 2, 4)),
-            dma((4, 32)),
+            dma((4, 26)),
             dma((2,)),
             dma((8,)),
             dma((8,)),
             dma((8,)),
             dma((8,)),
             dma((2,)),
-            dma((4, 2)),
-            dma((4, 2)),
+            dma((3, 2)),
+            dma((3, 2)),
         ],
         compiler_params=pltpu.CompilerParams(
             collective_id=0, has_side_effects=True, vmem_limit_bytes=56 * 1024 * 1024

time: 82.9 us -> 81.6 us (0.984)
  the two profiles are of different devices: /device:TPU:3 before, /device:TPU:21 now
where the time goes in v4:
time: 81.6 us; the launch traced here: 81.4 us
  Pallas kernels  79.6 us (98%)
  local copies, waits for them, and re-layouts  1.77 us (2%)
    pallas_call x1, Pallas kernels, body(): pl.pallas_call(kernel, out_shape=jax.ShapeDtypeStruct((768, 256), BF16),...  79.6 us
    unnamed x1, local copies, waits for them, and re-layouts  1.77 us

profile of v4, /device:TPU:21, one launch (start us, length us, event | category | flops | bytes accessed | tf_op | source)
XLA Modules:
  0.0 81.4 jit_solution(10355966962663017926)
XLA Ops:
  0.0 79.6 %shard_map.82 = bf16[768,256]{1,0:T(8,128)(2,1)} custom-call(bf16[768,2048]{1,0:T(8,128)(2,1)} %tokens.1, f32[1,2048]{1,0:T(1,128)} %bitcast.4, f32[32,704]{1,0:T(8,128)} %gate_w.1, f32[32,704]{1,0:T(8,128)} %up_w.1, f32[704]{0:T(1024)} %gate_s.1, f32[704]{0:T(1024)} %up_s.1, f32[32,704]{1,0:T(8,128)} %bitcast.3, f32[1,256]{1,0:T(1,128)} %bitcast.5), custom_call_target="tpu_custom_call" | custom-call | tf_op jit(solution)/shard_map/pallas_call | solution.py:455
  79.6 1.8 %copy.10 = bf16[768,256]{1,0:T(8,128)(2,1)} copy(bf16[768,256]{1,0:T(8,128)(2,1)} %shard_map.82) | data formatting | bytes 786432

commit v5 on v4

--- a/solution.py
+++ b/solution.py
@@ -34,8 +34,7 @@
     def second(self, way, hop, j, source):
         at = self.buf.at[wrap(self.major + source), wrap(self.minor + OFF[j])]
         if hop == 4:
-            half = self.buf.shape[2] // 2
-            at = at.at[pl.ds(way * half, half)]
+            at = at.at[self.half(way)]
         return pltpu.make_async_remote_copy(
             src_ref=at, dst_ref=at, send_sem=self.send2, recv_sem=self.recv2.at[self.number(way, hop, j // self.sizes[hop - 1])],
             device_id=self.along_major[way], device_id_type=MESH,
@@ -45,6 +44,10 @@
         self.first(PLUS, 1, 0).start()
         self.first(MINUS, 1, 0).start()
 
+    def half(self, way):
+        length = self.buf.shape[2]
+        return pl.ds(0, length // 2) if way == PLUS else pl.ds(length // 2, length - length // 2)
+
     def send(self, way, j):
         self.second(way, 1, j, 0).start()
 
@@ -54,7 +57,9 @@
 
     def arrive(self, way, hop, group):
         size = self.sizes[hop - 1]
-        here = self.buf.at[0, pl.ds(0, size if hop < 4 else size // 2)]
+        here = self.buf.at[0, pl.ds(0, size)]
+        if hop == 4:
+            here = self.buf.at[0, pl.ds(0, size), self.half(way)]
         pltpu.make_async_copy(here, here, self.recv2.at[self.number(way, hop, group)]).wait()
 
     def line(self, step):
@@ -144,9 +149,12 @@
         for way in (PLUS, MINUS):
             g.send(way, 0)
     fetches[2].wait()
-    turned = jnp.concatenate([dw_in[...], jnp.zeros((32, 64), F32)], axis=1).astype(BF16)
-    buf_c[z, y] = turned[0:16]
-    buf_d[y, z] = turned[16:32]
+    for top, place_of in ((0, buf_c.at[z, y]), (16, buf_d.at[y, z])):
+        upper, lower = dw_in[top : top + 8, :], dw_in[top + 8 : top + 16, :]
+        for k in range(5):
+            place_of[2 * k] = upper[:, k * 128 : k * 128 + 128].astype(BF16)
+            place_of[2 * k + 1] = lower[:, k * 128 : k * 128 + 128].astype(BF16)
+        place_of[10] = jnp.concatenate([upper[:, 640:], lower[:, 640:]], axis=1).astype(BF16)
     for g in deep:
         g.start_first()
     for g in deep:
@@ -287,7 +295,11 @@
         sign = 1 if block % 2 == 0 else -1
         group = block // 2
         at = wrap((z, y)[group] + sign * away)
-        left = (buf_c, buf_d)[group][at].reshape(128, 768)
+        tiles = (buf_c, buf_d)[group]
+        upper = tiles[at, :, 10].astype(F32)
+        lower = pltpu.roll(upper.reshape(64, 128), 64, 1).reshape(8, 8, 128)
+        last = jnp.stack([upper, lower], axis=1).reshape(128, 128).astype(BF16)
+        left = jnp.concatenate([tiles[at, :, 2 * k : 2 * k + 2].reshape(128, 128) for k in range(5)] + [last], axis=1)
         part = jnp.dot(left, half_of(core if mine else other), preferred_element_type=F32)
         if mine:
             (own_a, own_b)[group][at] = part
@@ -470,8 +482,8 @@
             pltpu.VMEM((2, 8, 768, 256), BF16),
             pltpu.VMEM((8, 8, 32, 768), BF16),
             pltpu.VMEM((8, 8, 32, 640), BF16),
-            pltpu.VMEM((8, 8, 16, 768), BF16),
-            pltpu.VMEM((8, 8, 16, 768), BF16),
+            pltpu.VMEM((8, 8, 11, 8, 128), BF16),
+            pltpu.VMEM((8, 8, 11, 8, 128), BF16),
             pltpu.VMEM((768, 768), F32),
             pltpu.VMEM((768, 640), F32),
             pltpu.VMEM((6, 768, 128), BF16),

time: 81.6 us -> 80.8 us (level)
  no operation moved by 1% of the time
where the time goes in v5:
time: 80.8 us; the launch traced here: 80.6 us
  Pallas kernels  78.8 us (98%)
  local copies, waits for them, and re-layouts  1.77 us (2%)
    pallas_call x1, Pallas kernels, body(): pl.pallas_call(kernel, out_shape=jax.ShapeDtypeStruct((768, 256), BF16),...  78.8 us
    unnamed x1, local copies, waits for them, and re-layouts  1.77 us

profile of v5, /device:TPU:21, one launch (start us, length us, event | category | flops | bytes accessed | tf_op | source)
XLA Modules:
  0.0 80.6 jit_solution(26815551694200063)
XLA Ops:
  0.0 78.8 %shard_map.82 = bf16[768,256]{1,0:T(8,128)(2,1)} custom-call(bf16[768,2048]{1,0:T(8,128)(2,1)} %tokens.1, f32[1,2048]{1,0:T(1,128)} %bitcast.4, f32[32,704]{1,0:T(8,128)} %gate_w.1, f32[32,704]{1,0:T(8,128)} %up_w.1, f32[704]{0:T(1024)} %gate_s.1, f32[704]{0:T(1024)} %up_s.1, f32[32,704]{1,0:T(8,128)} %bitcast.3, f32[1,256]{1,0:T(1,128)} %bitcast.5), custom_call_target="tpu_custom_call" | custom-call | tf_op jit(solution)/shard_map/pallas_call | solution.py:467
  78.8 1.8 %copy.10 = bf16[768,256]{1,0:T(8,128)(2,1)} copy(bf16[768,256]{1,0:T(8,128)(2,1)} %shard_map.82) | data formatting | bytes 786432

commit v6 on v5

--- a/solution.py
+++ b/solution.py
@@ -11,7 +11,7 @@
 F32, BF16 = jnp.float32, jnp.bfloat16
 OFF = (0, 1, -1, 2, -2, 3, -3, 4)
 PLUS, MINUS = 0, 1
-WIDE, DEEP = (2, 4, 4, 4), (2, 2, 2, 8)
+WIDE, DEEP = (2, 4, 4, 8), (2, 2, 2, 8)
 
 
 def wrap(i):
@@ -89,7 +89,7 @@
     tokens, gain, gate_w, up_w, gate_s, up_s, down_w, down_s, out,
     tok, gw_in, uw_in, dw_in, gain_in, gs_in, us_in, ds_in, perm, x_all, buf_a, buf_b, buf_c, buf_d, acc_a, acc_b, hid,
     own_a, own_b, give_a, give_b, got_a, got_b, sum_a, sum_b, via_a, via_b, all_a, all_b, flat,
-    in_sem, send1, send2, recv1, recv2, pair_send, pair_a, pair_b, via_a_sem, via_b_sem, x_send, x_a_sem, x_b_sem,
+    in_sem, send1, send2, recv1, recv2, pair_send, pair_recv, via_a_sem, via_b_sem, x_send, x_a_sem, x_b_sem,
 ):
     z, y, tp = lax.axis_index("fs_0"), lax.axis_index("fs_1"), lax.axis_index("tp")
     core = lax.rem(tp, 2)
@@ -252,8 +252,8 @@
     for group in range(2):
         for p in range(4 * group, 4 * group + 4):
             wide_piece(p, 3)
-        for g in wide:
-            g.hop(4, group)
+    for g in wide:
+        g.hop(4, 0)
     for p in (0, 1, 4, 5):
         wide_piece(p, 4)
 
@@ -278,15 +278,15 @@
         hid[k] = h.T.astype(BF16)
         return 0
 
-    lax.fori_loop(0, 6, activate, 0)
+    lax.fori_loop(0, 6, activate, 0, unroll=2)
 
     def half_of(which):
         return jnp.concatenate([hid[which * 3 + k] for k in range(3)], axis=1)
 
-    def exchange(group, at):
-        give, got, sem = (give_a, got_a, pair_a) if group == 0 else (give_b, got_b, pair_b)
+    def exchange(group, at, away):
+        give, got = (give_a, got_a) if group == 0 else (give_b, got_b)
         return pltpu.make_async_remote_copy(
-            src_ref=give.at[at], dst_ref=got.at[at], send_sem=pair_send.at[group], recv_sem=sem.at[at],
+            src_ref=give.at[at], dst_ref=got.at[at], send_sem=pair_send.at[group], recv_sem=pair_recv.at[away],
             device_id={"tp": peer}, device_id_type=MESH,
         )
 
@@ -305,7 +305,7 @@
             (own_a, own_b)[group][at] = part
         else:
             (give_a, give_b)[group][at] = part.astype(BF16)
-            exchange(group, at).start()
+            exchange(group, at, away).start()
 
     def put(group, src, slot, row, owner):
         dst, sem = (all_a.at[slot, core], x_a_sem) if group == 0 else (all_b.at[slot, core, row], x_b_sem)
@@ -325,7 +325,6 @@
     added_slot = 1 + core
 
     def combine_one(group, at):
-        exchange(group, at).wait_recv()
         if group == 0:
             total = own_a[at] + got_a[at].astype(F32)
             low = total.astype(BF16).reshape(8, 16, 384)
@@ -387,6 +386,8 @@
                 act(group, wrap(me - away))
 
     def combine(away):
+        landed = got_a.at[pl.ds(0, 4 if 0 < away < 4 else 2)]
+        pltpu.make_async_copy(landed, landed, pair_recv.at[away]).wait()
         both_sides(combine_one, away)
 
     def finish(away):
@@ -506,8 +507,7 @@
             dma((4, 2, 4)),
             dma((4, 26)),
             dma((2,)),
-            dma((8,)),
-            dma((8,)),
+            dma((5,)),
             dma((8,)),
             dma((8,)),
             dma((2,)),

time: 80.8 us -> 81.1 us (level)
  no operation moved by 1% of the time
where the time goes in v6:
time: 81.1 us; the launch traced here: 80.9 us
  Pallas kernels  79.1 us (98%)
  local copies, waits for them, and re-layouts  1.77 us (2%)
    pallas_call x1, Pallas kernels, body(): pl.pallas_call(kernel, out_shape=jax.ShapeDtypeStruct((768, 256), BF16),...  79.1 us
    unnamed x1, local copies, waits for them, and re-layouts  1.77 us

profile of v6, /device:TPU:21, one launch (start us, length us, event | category | flops | bytes accessed | tf_op | source)
XLA Modules:
  0.0 80.9 jit_solution(17381665410507064917)
XLA Ops:
  0.0 79.1 %shard_map.82 = bf16[768,256]{1,0:T(8,128)(2,1)} custom-call(bf16[768,2048]{1,0:T(8,128)(2,1)} %tokens.1, f32[1,2048]{1,0:T(1,128)} %bitcast.4, f32[32,704]{1,0:T(8,128)} %gate_w.1, f32[32,704]{1,0:T(8,128)} %up_w.1, f32[704]{0:T(1024)} %gate_s.1, f32[704]{0:T(1024)} %up_s.1, f32[32,704]{1,0:T(8,128)} %bitcast.3, f32[1,256]{1,0:T(1,128)} %bitcast.5), custom_call_target="tpu_custom_call" | custom-call | tf_op jit(solution)/shard_map/pallas_call | solution.py:468
  79.2 1.8 %copy.10 = bf16[768,256]{1,0:T(8,128)(2,1)} copy(bf16[768,256]{1,0:T(8,128)(2,1)} %shard_map.82) | data formatting | bytes 786432
